TPU v7x, 32 devices: a whole 2x2x4 slice. The times are simulated.
32 devices in a mesh: fs: 8 (over z, y), tp: 4 (over x, core).
Axes of the slice: x: 2, y: 2, z: 4, core: 2. Of those that a mesh axis runs over, the one named last changes fastest.
Arguments:
- tokens: bfloat16 [6144, 2048], P(('fs', 'tp')), may hold values from -60 to 60
- norm_gain: float32 [2048], P('fs'), may hold values from 0.1 to 1.9
- gate_weight: float32 [2048, 5632], P('fs', 'tp'), may hold values from -0.125 to 0.125
- up_weight: float32 [2048, 5632], P('fs', 'tp'), may hold values from -0.125 to 0.125
- down_weight: float32 [2048, 5632], P('fs', 'tp'), may hold values from -0.078125 to 0.078125
Outputs:
- mixed_rows: bfloat16 [6144, 2048], P(('fs', 'tp'))
- gate_out: bfloat16 [2048, 5632], P(None, 'tp')
- up_out: bfloat16 [2048, 5632], P(None, 'tp')
- down_out: bfloat16 [2048, 5632], P(None, 'tp')
All inputs are finite; a program needn't handle non-finite values.
Results may differ from a plain program's by a relative error of at most 0.014.
Values may be sent and summed in bfloat16 or wider, within the bound.
A program may use at most 128 MiB of HBM per device.

v0:
```python
import jax
import jax.numpy as jnp
from jax import lax
from jax.sharding import PartitionSpec as P


def normalize(source):
    widened = source.astype(jnp.float32)
    return (widened * lax.rsqrt(jnp.mean(widened * widened, axis=1, keepdims=True) + 1e-06)).astype(
        jnp.bfloat16
    )


def shards(tokens, norm_gain, gate_weight, up_weight, down_weight):
    row_gain = norm_gain[:, None]
    gate_local = (gate_weight * row_gain).astype(jnp.bfloat16)
    up_local = (up_weight * row_gain).astype(jnp.bfloat16)
    down_local = down_weight.astype(jnp.bfloat16)
    normed = normalize(tokens)
    gathered = lax.all_gather(normed, "tp", axis=0, tiled=True)
    down_whole = lax.all_gather(down_local, "fs", axis=0, tiled=True)
    gate_piece = lax.all_gather(gate_local, "fs", axis=0, tiled=True)
    up_piece = lax.all_gather(up_local, "fs", axis=0, tiled=True)
    gate_acc = jnp.dot(gathered, gate_piece, preferred_element_type=jnp.float32)
    up_acc = jnp.dot(gathered, up_piece, preferred_element_type=jnp.float32)
    hidden = (jax.nn.silu(gate_acc) * up_acc).astype(jnp.bfloat16)
    partial_value = lax.dot_general(
        hidden, down_whole, (((1,), (1,)), ((), ())), preferred_element_type=jnp.float32
    )
    mixed_rows = lax.psum_scatter(
        lax.optimization_barrier(partial_value.astype(jnp.bfloat16))
        .astype(jnp.float32)
        .astype(jnp.bfloat16),
        "tp",
        scatter_dimension=0,
        tiled=True,
    )
    return (mixed_rows, gate_piece, up_piece, down_whole)


def solution(mesh):
    in_specs = (P(("fs", "tp"), None), P("fs"), P("fs", "tp"), P("fs", "tp"), P("fs", "tp"))
    out_specs = (P(("fs", "tp"), None), P(None, "tp"), P(None, "tp"), P(None, "tp"))
    return jax.shard_map(shards, mesh=mesh, in_specs=in_specs, out_specs=out_specs, check_vma=False)
```

profile of v0, /device:TPU:0, one launch (start us, length us, event | category | flops | bytes accessed | tf_op | source)
XLA Modules:
  0.0 397.9 jit_solution(9030108663980922372)
XLA Ops:
  7.2 0.0 copy-start
  7.2 0.0 all-gather.5.cloned.1.call-start
  7.2 1.5 fusion
  8.7 2.2 fusion.1
  10.9 0.0 all-gather.5.cloned.1.call-update
  10.9 0.0 all-gather.7.cloned.1.call-start
  11.0 3.2 multiply_convert_fusion.1
  14.2 0.0 all-gather.7.cloned.1.call-update
  14.2 0.0 all-gather.11.cloned.1.call-start
  14.2 0.0 copy-done
  14.2 0.9 convert_element_type.28
  15.2 0.0 all-gather.11.cloned.1.call-update
  15.2 0.0 all-gather.9.cloned.1.call-start
  15.3 0.5 all-gather.9.cloned.1.call-update
  15.8 0.0 reduce-scatter.2.cloned.1.call-start
  15.8 26.5 %all-gather.5.cloned.1.call-done = bf16[768,2048]{1,0:T(8,128)(2,1)} async-done(((bf16[192,2048]{1,0:T(8,128)(2,1)}), bf16[768,2048]{1,0:T(8,128)(2,1)}) %all-gather.5.cloned.1.call-update) | async-done | bytes 3145744 | tf_op jit(solution)/shard_map/all_gather | solution.py:20
  42.3 0.0 copy-start.1
  42.3 95.1 %all-gather.7.cloned.1.call-done = bf16[2048,1408]{1,0:T(8,128)(2,1)} async-done(((bf16[256,1408]{1,0:T(8,128)(2,1)}), bf16[2048,1408]{1,0:T(8,128)(2,1)}) %all-gather.7.cloned.1.call-update) | async-done | bytes 5767184 | tf_op jit(solution)/shard_map/all_gather | solution.py:22
  137.4 9.7 %fusion.3 = f32[768,1408]{1,0:T(8,128)} fusion(bf16[768,2048]{1,0:T(8,128)(2,1)} %all-gather.5.cloned.1.call-done, bf16[2048,1408]{1,0:T(8,128)(2,1)} %all-gather.7.cloned.1.call-done), kind=kOutput, calls=%fused_computation.10 | convolution fusion | flops 4429185024 | bytes 13238272 | tf_op jit(solution)/shard_map/dot_general | solution.py:24
  147.1 83.6 %all-gather.11.cloned.1.call-done = bf16[2048,1408]{1,0:T(8,128)(2,1)} async-done(((bf16[256,1408]{1,0:T(8,128)(2,1)}), bf16[2048,1408]{1,0:T(8,128)(2,1)}) %all-gather.11.cloned.1.call-update) | async-done | bytes 5767184 | tf_op jit(solution)/shard_map/all_gather | solution.py:21
  230.7 93.1 %all-gather.9.cloned.1.call-done = bf16[2048,1408]{1,0:T(8,128)(2,1)} async-done(((bf16[256,1408]{1,0:T(8,128)(2,1)}), bf16[2048,1408]{1,0:T(8,128)(2,1)}) %all-gather.9.cloned.1.call-update) | async-done | bytes 5767184 | tf_op jit(solution)/shard_map/all_gather | solution.py:23
  323.8 0.0 copy-done.1
  323.8 17.3 %convolution_convert_fusion = bf16[768,2048]{1,0:T(8,128)(2,1)} fusion(bf16[2048,1408]{1,0:T(8,128)(2,1)} %all-gather.11.cloned.1.call-done, f32[768,1408]{1,0:T(8,128)} %fusion.3, bf16[768,2048]{1,0:T(8,128)(2,1)S(1)} %copy-done.1, bf16[2048,1408]{1,0:T(8,128)(2,1)} %all-gather.9.cloned.1.call-done), kind=kOutput, calls=%fused_computation.1 | convolution fusion | flops 8866430976 | bytes 22151168 | tf_op jit(solution)/shard_map/dot_general | solution.py:27
  341.2 0.0 reduce-scatter.2.cloned.1.call-update
  341.2 36.2 %reduce-scatter.2.cloned.1.call-done = bf16[192,2048]{1,0:T(8,128)(2,1)} async-done(((bf16[768,2048]{1,0:T(8,128)(2,1)}), bf16[192,2048]{1,0:T(8,128)(2,1)}) %reduce-scatter.2.cloned.1.call-update) | async-done | bytes 786448 | tf_op jit(solution)/shard_map/reduce_scatter | solution.py:30
  377.4 0.0 slice-start
  377.4 5.7 %copy.12 = bf16[2048,1408]{1,0:T(8,128)(2,1)} copy(bf16[2048,1408]{1,0:T(8,128)(2,1)} %all-gather.7.cloned.1.call-done) | data formatting | bytes 11534336
  383.2 0.0 slice-start.1
  383.2 5.7 %copy.13 = bf16[2048,1408]{1,0:T(8,128)(2,1)} copy(bf16[2048,1408]{1,0:T(8,128)(2,1)} %all-gather.9.cloned.1.call-done) | data formatting | bytes 11534336
  388.9 0.0 slice-done
  388.9 0.0 slice-done.1
  388.9 2.5 copy.14
  (2 shorter events, 0.0 us)
Async XLA Ops:
  7.2 7.1 %copy-start = (f32[256,1408]{1,0:T(8,128)S(1)}, f32[256,1408]{1,0:T(8,128)}, u32[]{:S(2)}) copy-start(f32[256,1408]{1,0:T(8,128)} %param.9) | copy-start | bytes 4325380
  7.2 35.2 %all-gather.5.cloned.1.call-start = ((), (), s32[]{:S(2)}) async-start(), calls=%async_computation.1 | async-start | bytes 3932160 | tf_op jit(solution)/shard_map/all_gather | solution.py:20
  10.9 126.5 %all-gather.7.cloned.1.call-start = ((), (), s32[]{:S(2)}) async-start(), calls=%async_computation.2 | async-start | bytes 6488064 | tf_op jit(solution)/shard_map/all_gather | solution.py:22
  14.2 216.5 %all-gather.11.cloned.1.call-start = ((), (), s32[]{:S(2)}) async-start(), calls=%async_computation.4 | async-start | bytes 6488064 | tf_op jit(solution)/shard_map/all_gather | solution.py:21
  15.2 308.6 %all-gather.9.cloned.1.call-start = ((), (), s32[]{:S(2)}) async-start(), calls=%async_computation.3 | async-start | bytes 6488064 | tf_op jit(solution)/shard_map/all_gather | solution.py:23
  15.8 361.6 %reduce-scatter.2.cloned.1.call-start = ((), (), s32[]{:S(2)}) async-start(), calls=%async_computation.5 | async-start | bytes 3932160 | tf_op jit(solution)/shard_map/reduce_scatter | solution.py:30
  42.3 281.5 %copy-start.1 = (bf16[768,2048]{1,0:T(8,128)(2,1)S(1)}, bf16[768,2048]{1,0:T(8,128)(2,1)}, u32[]{:S(2)}) copy-start(bf16[768,2048]{1,0:T(8,128)(2,1)} %all-gather.5.cloned.1.call-done) | copy-start | bytes 9437188
  377.4 11.5 %slice-start = ((s8[5767168]{0:T(1024)(128)(4,1)}), s8[4194304]{0:T(1024)(128)(4,1)S(1)}, s32[]{:S(2)}) async-start(s8[5767168]{0:T(1024)(128)(4,1)} %bitcast.5), calls=%async_computation.6 | async-start | bytes 8388608
  383.2 5.7 %slice-start.1 = ((s8[5767168]{0:T(1024)(128)(4,1)}), s8[1572864]{0:T(1024)(128)(4,1)S(1)}, s32[]{:S(2)}) async-start(s8[5767168]{0:T(1024)(128)(4,1)} %bitcast.5), calls=%async_computation.7 | async-start | bytes 3145728
Sparse Core Ops, SparseCore 0:
  11.1 31.2 all-gather.4
  45.1 92.2 all-gather.6
  140.2 90.4 all-gather.10
  233.3 90.4 all-gather.8
  341.3 36.0 reduce-scatter.1
where the time goes:
time: 398 us
  waiting for transfers between devices  335 us (84%)
  matrix products  27 us (7%)
  local copies, waits for them, and re-layouts  14 us (4%)
  between operations  13.8 us (3%)
  other arithmetic  7.8 us (2%)
    all_gather x1, waiting for transfers between devices, shards(): gate_piece = lax.all_gather(gate_local, 'fs', axis=0, tiled=True)  95.1 us
    all_gather x1, waiting for transfers between devices, shards(): up_piece = lax.all_gather(up_local, 'fs', axis=0, tiled=True)  93.1 us
    all_gather x1, waiting for transfers between devices, shards(): down_whole = lax.all_gather(down_local, 'fs', axis=0, tiled=True)  83.6 us
    reduce_scatter x1, waiting for transfers between devices, shards(): lax.psum_scatter(lax.optimization_barrier(partial_value.astype(jnp.bfloat...  36.2 us
    all_gather x1, waiting for transfers between devices, shards(): gathered = lax.all_gather(normed, 'tp', axis=0, tiled=True)  26.5 us
    dot_general x1, matrix products, shards(): lax.dot_general(hidden, down_whole, (((1,), (1,)), ((), ())), preferred_e...  17.3 us
    unnamed x11, local copies, waits for them, and re-layouts  14 us
    dot_general x1, matrix products, shards(): gate_acc = jnp.dot(gathered, gate_piece, preferred_element_type=jnp.float32)  9.67 us
  transfers between devices with their start and end apart: 5, of which 5 were waited for; matrix products, arithmetic and copies ran while one was open for 3% of the time, Pallas kernels for 0%

commit v1 on v0

--- a/solution.py
+++ b/solution.py
@@ -19,8 +19,11 @@
     normed = normalize(tokens)
     gathered = lax.all_gather(normed, "tp", axis=0, tiled=True)
     down_whole = lax.all_gather(down_local, "fs", axis=0, tiled=True)
-    gate_piece = lax.all_gather(gate_local, "fs", axis=0, tiled=True)
-    up_piece = lax.all_gather(up_local, "fs", axis=0, tiled=True)
+    gate_piece, up_piece = jnp.split(
+        jax.lax.all_gather(jnp.concatenate([gate_local, up_local], 1), "fs", tiled=True, axis=0),
+        [gate_local.shape[1]],
+        1,
+    )
     gate_acc = jnp.dot(gathered, gate_piece, preferred_element_type=jnp.float32)
     up_acc = jnp.dot(gathered, up_piece, preferred_element_type=jnp.float32)
     hidden = (jax.nn.silu(gate_acc) * up_acc).astype(jnp.bfloat16)

time: 398 us -> 366 us (0.920)
  waiting for transfers between devices: 335 us -> 304 us
    all_gather x2 -> x1, waiting for transfers between devices: 188 us -> 164 us  [shards(): jax.lax.all_gather(jnp.concatenate([gate_local, up_local], 1), 'fs', tile...]
    split x0 -> x1, local copies, waits for them, and re-layouts: none -> 9.89 us  [shards(): jnp.split(jax.lax.all_gather(jnp.concatenate([gate_local, up_local], 1),...]
    unnamed x11 -> x7, local copies, waits for them, and re-layouts: 14 us -> 5.68 us
    all_gather x1, waiting for transfers between devices: 26.5 us -> 19 us  [shards(): gathered = lax.all_gather(normed, 'tp', axis=0, tiled=True)]
  transfers between devices with their start and end apart: 5 -> 4, of which waited for: 5 -> 4; matrix products, arithmetic and copies ran while one was open for 3% -> 6% of each run, Pallas kernels for 0% -> 0%
where the time goes in v1:
time: 366 us
  waiting for transfers between devices  304 us (83%)
  matrix products  27.1 us (7%)
  local copies, waits for them, and re-layouts  15.6 us (4%)
  between operations  13.8 us (4%)
  other arithmetic  5.54 us (2%)
    all_gather x1, waiting for transfers between devices, shards(): jax.lax.all_gather(jnp.concatenate([gate_local, up_local], 1), 'fs', tile...  164 us
    all_gather x1, waiting for transfers between devices, shards(): down_whole = lax.all_gather(down_local, 'fs', axis=0, tiled=True)  84.7 us
    reduce_scatter x1, waiting for transfers between devices, shards(): lax.psum_scatter(lax.optimization_barrier(partial_value.astype(jnp.bfloat...  36.2 us
    all_gather x1, waiting for transfers between devices, shards(): gathered = lax.all_gather(normed, 'tp', axis=0, tiled=True)  19 us
    dot_general x1, matrix products, shards(): lax.dot_general(hidden, down_whole, (((1,), (1,)), ((), ())), preferred_e...  17.3 us
    split x1, local copies, waits for them, and re-layouts, shards(): jnp.split(jax.lax.all_gather(jnp.concatenate([gate_local, up_local], 1),...  9.89 us
    dot_general x1, matrix products, shards(): gate_acc = jnp.dot(gathered, gate_piece, preferred_element_type=jnp.float32)  9.8 us
  transfers between devices with their start and end apart: 4, of which 4 were waited for; matrix products, arithmetic and copies ran while one was open for 6% of the time, Pallas kernels for 0%

profile of v1, /device:TPU:0, one launch (start us, length us, event | category | flops | bytes accessed | tf_op | source)
XLA Modules:
  0.0 365.8 jit_solution(17747635171327998706)
XLA Ops:
  7.2 0.0 all-gather.6.cloned.1.call-start
  7.2 2.1 multiply_convert_fusion.2
  9.3 0.0 copy-start
  9.3 0.0 copy-start.1
  9.3 1.2 pad_maximum_fusion
  10.5 0.0 all-gather.6.cloned.1.call-update
  10.5 0.0 all-gather.4.cloned.1.call-start
  10.6 0.1 copy-done
  10.7 0.2 fusion
  10.9 1.1 fusion.1
  12.0 0.0 all-gather.4.cloned.1.call-update
  12.0 0.0 all-gather.8.cloned.1.call-start
  12.1 0.0 copy-done.1
  12.1 0.9 convert_element_type.28
  13.0 0.0 all-gather.8.cloned.1.call-update
  13.0 0.0 reduce-scatter.2.cloned.1.call-start
  13.1 163.7 %all-gather.6.cloned.1.call-done = bf16[2048,2816]{1,0:T(8,128)(2,1)} async-done(((bf16[256,2816]{1,0:T(8,128)(2,1)}), bf16[2048,2816]{1,0:T(8,128)(2,1)}) %all-gather.6.cloned.1.call-update) | async-done | bytes 11534352 | tf_op jit(solution)/shard_map/all_gather | solution.py:23
  176.8 9.9 %fusion.3 = (bf16[2048,1408]{1,0:T(8,128)(2,1)}, bf16[2048,1408]{1,0:T(8,128)(2,1)}) fusion(bf16[2048,2816]{1,0:T(8,128)(2,1)} %all-gather.6.cloned.1.call-done), kind=kLoop, calls=%fused_computation.11 | loop fusion | bytes 23068672 | tf_op jit(solution)/shard_map/split | solution.py:22
  186.7 19.0 %all-gather.4.cloned.1.call-done = bf16[768,2048]{1,0:T(8,128)(2,1)} async-done(((bf16[192,2048]{1,0:T(8,128)(2,1)}), bf16[768,2048]{1,0:T(8,128)(2,1)}) %all-gather.4.cloned.1.call-update) | async-done | bytes 3145744 | tf_op jit(solution)/shard_map/all_gather | solution.py:20
  205.7 0.0 copy-start.2
  205.7 9.8 %fusion.4 = f32[768,1408]{1,0:T(8,128)} fusion(bf16[768,2048]{1,0:T(8,128)(2,1)} %all-gather.4.cloned.1.call-done, bf16[2048,1408]{1,0:T(8,128)(2,1)} %get-tuple-element.13), kind=kOutput, calls=%fused_computation.12 | convolution fusion | flops 4429185024 | bytes 13238272 | tf_op jit(solution)/shard_map/dot_general | solution.py:27
  215.5 84.7 %all-gather.8.cloned.1.call-done = bf16[2048,1408]{1,0:T(8,128)(2,1)} async-done(((bf16[256,1408]{1,0:T(8,128)(2,1)}), bf16[2048,1408]{1,0:T(8,128)(2,1)}) %all-gather.8.cloned.1.call-update) | async-done | bytes 5767184 | tf_op jit(solution)/shard_map/all_gather | solution.py:21
  300.2 0.0 copy-done.2
  300.2 17.3 %convolution_convert_fusion = bf16[768,2048]{1,0:T(8,128)(2,1)} fusion(bf16[2048,1408]{1,0:T(8,128)(2,1)} %all-gather.8.cloned.1.call-done, f32[768,1408]{1,0:T(8,128)} %fusion.4, bf16[768,2048]{1,0:T(8,128)(2,1)S(1)} %copy-done.2, bf16[2048,1408]{1,0:T(8,128)(2,1)} %get-tuple-element.14), kind=kOutput, calls=%fused_computation.1 | convolution fusion | flops 8866430976 | bytes 22151168 | tf_op jit(solution)/shard_map/dot_general | solution.py:30
  317.5 0.0 reduce-scatter.2.cloned.1.call-update
  317.5 36.2 %reduce-scatter.2.cloned.1.call-done = bf16[192,2048]{1,0:T(8,128)(2,1)} async-done(((bf16[768,2048]{1,0:T(8,128)(2,1)}), bf16[192,2048]{1,0:T(8,128)(2,1)}) %reduce-scatter.2.cloned.1.call-update) | async-done | bytes 786448 | tf_op jit(solution)/shard_map/reduce_scatter | solution.py:33
  353.7 5.6 %copy.10 = bf16[2048,1408]{1,0:T(8,128)(2,1)} copy(bf16[2048,1408]{1,0:T(8,128)(2,1)} %all-gather.8.cloned.1.call-done) | data formatting | bytes 11534336
  (1 shorter events, 0.0 us)
Async XLA Ops:
  7.2 169.6 %all-gather.6.cloned.1.call-start = ((), (), s32[]{:S(2)}) async-start(), calls=%async_computation.2 | async-start | bytes 12976128 | tf_op jit(solution)/shard_map/all_gather | solution.py:23
  9.3 1.4 copy-start
  9.3 2.8 copy-start.1
  10.5 195.1 %all-gather.4.cloned.1.call-start = ((), (), s32[]{:S(2)}) async-start(), calls=%async_computation.1 | async-start | bytes 3932160 | tf_op jit(solution)/shard_map/all_gather | solution.py:20
  12.0 288.2 %all-gather.8.cloned.1.call-start = ((), (), s32[]{:S(2)}) async-start(), calls=%async_computation.3 | async-start | bytes 6488064 | tf_op jit(solution)/shard_map/all_gather | solution.py:21
  13.0 340.7 %reduce-scatter.2.cloned.1.call-start = ((), (), s32[]{:S(2)}) async-start(), calls=%async_computation.4 | async-start | bytes 3932160 | tf_op jit(solution)/shard_map/reduce_scatter | solution.py:33
  205.7 94.5 %copy-start.2 = (bf16[768,2048]{1,0:T(8,128)(2,1)S(1)}, bf16[768,2048]{1,0:T(8,128)(2,1)}, u32[]{:S(2)}) copy-start(bf16[768,2048]{1,0:T(8,128)(2,1)} %all-gather.4.cloned.1.call-done) | copy-start | bytes 9437188
Sparse Core Ops, SparseCore 0:
  10.7 166.0 all-gather.5
  178.9 26.6 all-gather.3
  207.8 92.2 all-gather.7
  317.6 36.0 reduce-scatter.1
